TPU v7x, 32 devices: a whole 2x2x4 slice. The times are simulated.
32 devices in a mesh: grp: 2 (over x), sp: 8 (over z, y), tp: 2 (over core).
Axes of the slice: x: 2, y: 2, z: 4, core: 2. Of those that a mesh axis runs over, the one named last changes fastest.
Arguments:
- tokens: bfloat16 [8192, 2048], P(('grp', 'sp', 'tp')), parts along dimension 0, may hold values from -64 to 64
- w_query: bfloat16 [2048, 1024], P(None, 'tp'), may hold values from -0.125 to 0.125
- w_key: bfloat16 [2048, 1024], P(None, 'tp'), may hold values from -0.125 to 0.125
- w_value: bfloat16 [2048, 1024], P(None, 'tp'), may hold values from -0.25 to 0.25
- w_out: bfloat16 [1024, 2048], P('tp'), may hold values from -0.1875 to 0.1875
Outputs:
- mixed: bfloat16 [8192, 2048], P(('grp', 'sp', 'tp')), parts along dimension 0
- log_sums: float32 [16, 8192], P('tp', ('grp', 'sp')), parts along dimension 1
There are 2 independent parts, one for each index of `grp`. A program takes and returns all parts, laid end to end along the dimension named above; an argument that names none is the same for every part. Nothing has to cross between parts.
All inputs are finite; a program needn't handle non-finite values.
Results may differ from a plain program's by a relative error of at most 0.013.
The roundings to bfloat16 on the way count: a program that leaves them out, or rounds other values in their place, can miss the bound.
Values may be sent and summed in bfloat16 or wider, within the bound.
A program may use at most 128 MiB of HBM per device.

v0:
```python
import functools
import math

import jax
import jax.numpy as jnp
from jax import lax
from jax.experimental import pallas as pl
from jax.experimental.pallas import tpu as pltpu
from jax.sharding import PartitionSpec as P

HEADS = 16
HEAD_DIM = 64
WINDOW_KEY_STEPS = 128
MIDDLE_DILATION = 4
FAR_DILATION = 16
REACH = 2048
ALIBI_EXP = 16.0
LANES = 128
F32 = jnp.float32
BF16 = jnp.bfloat16


def log_multiplicity(distance):
    def window(stride):
        inside = (distance >= 0) & (distance <= WINDOW_KEY_STEPS * stride)
        if stride > 1:
            inside = inside & ((distance & (stride - 1)) == 0)
        return inside.astype(jnp.int32)

    count = window(1) + window(MIDDLE_DILATION) + window(FAR_DILATION)
    return jnp.where(
        count == 3,
        math.log(3.0),
        jnp.where(count == 2, math.log(2.0), jnp.where(count == 1, 0.0, -jnp.inf)),
    ).astype(F32)


def kernel(
    n_sp,
    tokens,
    w_query,
    w_key,
    w_value,
    w_out,
    mixed,
    log_sums,
    x,
    wq,
    wk,
    wv,
    wo,
    nat,
    kbuf,
    vbuf,
    qz,
    half_perm,
    fwd_perm,
    back_perm,
    near_d,
    near_c,
    far_d,
    far_c,
    m_ref,
    l_ref,
    acc,
    hid,
    hid_nat,
    logs,
    part_sum,
    part_send,
    part_recv,
    local_sem,
    x_send,
    x_recv,
    kv_send,
    kv_recv,
    p_send,
    p_recv,
):
    half = tokens.shape[0]
    length = x.shape[0]
    n_slots, n_chunks = kbuf.shape[0], kbuf.shape[1]
    hops = n_slots - 1
    classes = MIDDLE_DILATION
    per = length // classes
    per_bits = per.bit_length() - 1
    me = lax.axis_index("sp")
    core = lax.axis_index("tp")
    other = 1 - core
    odd = lax.rem(me, 2)
    mate = me + 1 - 2 * odd

    my_rows = pl.ds(pl.multiple_of(core * half, half), half)
    their_rows = pl.ds(pl.multiple_of(other * half, half), half)
    local = [
        pltpu.make_async_copy(tokens, x.at[my_rows], local_sem.at[0]),
        pltpu.make_async_copy(w_key, wk, local_sem.at[1]),
        pltpu.make_async_copy(w_value, wv, local_sem.at[2]),
        pltpu.make_async_copy(w_query, wq, local_sem.at[3]),
        pltpu.make_async_copy(w_out, wo, local_sem.at[4]),
    ]
    for copy in local[:3]:
        copy.start()

    barrier = pltpu.get_barrier_semaphore()
    has_up = me + 2 < n_sp
    has_down = me >= 2
    pl.semaphore_signal(barrier, inc=1, device_id={"tp": other})
    pl.semaphore_signal(barrier, inc=1, device_id={"sp": mate})

    @pl.when(has_up)
    def _():
        pl.semaphore_signal(barrier, inc=1, device_id={"sp": me + 2})

    @pl.when(has_down)
    def _():
        pl.semaphore_signal(barrier, inc=1, device_id={"sp": me - 2})

    peers = 2 + jnp.where(has_up, 1, 0) + jnp.where(has_down, 1, 0)
    pl.semaphore_wait(barrier, peers)

    x_copy = pltpu.make_async_remote_copy(
        src_ref=tokens,
        dst_ref=x.at[my_rows],
        send_sem=x_send,
        recv_sem=x_recv,
        device_id={"tp": other},
    )
    x_copy.start()

    rows = lax.broadcasted_iota(jnp.int32, (length, length), 0)
    cols = lax.broadcasted_iota(jnp.int32, (length, length), 1)

    def time_of(place):
        return classes * (place & (per - 1)) + (place >> per_bits)

    half_rows = lax.broadcasted_iota(jnp.int32, (half, half), 0)
    half_cols = lax.broadcasted_iota(jnp.int32, (half, half), 1)
    half_time = classes * (half_rows & (per // 2 - 1)) + (half_rows >> (per_bits - 1))
    half_perm[...] = (half_time == half_cols).astype(F32).astype(BF16)

    def project(weights, which, rows_):
        nat[which, rows_, :] = jnp.dot(
            x[rows_, :], weights[...], preferred_element_type=F32
        ).astype(BF16)

    def hop(slot, c, kind):
        if slot % 2 == 0:
            source, target = slot - 2, me + 2
            target = jnp.where(has_up, target, me - 2)
        else:
            source, target = slot - 1 + 2 * odd, mate
        if kind == 0:
            late = c // (n_chunks // 2)
            side = core + late * (1 - 2 * core)
            pair = pl.ds(2 * (c - late * (n_chunks // 2)), 2)
            src, dst = kbuf.at[source, pair, :, side], kbuf.at[slot, pair, :, side]
        else:
            src, dst = vbuf.at[source, c], vbuf.at[slot, c]
        return pltpu.make_async_remote_copy(
            src_ref=src,
            dst_ref=dst,
            send_sem=kv_send.at[slot - 1, c, kind],
            recv_sem=kv_recv.at[slot - 1, c, kind],
            device_id={"sp": target},
        )

    def sends(slot):
        source = slot - 2 if slot % 2 == 0 else slot - 1 + 2 * odd
        holds = me >= source
        return holds & has_up if slot % 2 == 0 else holds

    def start(slot, c, kind, condition):
        @pl.when(condition & sends(slot))
        def _():
            hop(slot, c, kind).start()

    def arrive(slot, c, kind):
        hop(slot, c, kind).wait_recv()

    def arrive_keys(slot):
        @pl.loop(0, n_chunks)
        def _(c):
            arrive(slot, c, 0)

    is_even = odd == 0
    is_odd = odd == 1

    def forward(slot, c, kind):
        if slot + 2 <= hops:
            start(slot + 2, c, kind, me >= 0)
        if slot + 1 <= hops:
            start(slot + 1, c, kind, is_even)
        if slot >= 2:
            start(slot - 1, c, kind, is_odd)

    def place_keys(rows_, side):
        ordered = jnp.dot(half_perm[...], nat[0, rows_, :], preferred_element_type=F32)
        ordered = ordered.astype(BF16)
        for c in range(n_chunks):
            piece = ordered[:, c * LANES : (c + 1) * LANES]
            kbuf[0, c, :, side] = piece.reshape(classes, per // 2, LANES)

    local[0].wait()
    local[1].wait()
    project(wk, 0, my_rows)
    place_keys(my_rows, core)

    @pl.loop(0, n_chunks // 2)
    def _(c):
        forward(0, c, 0)

    local[2].wait()
    local[3].start()
    local[4].start()
    project(wv, 1, my_rows)
    fwd_perm[...] = (rows == time_of(cols)).astype(F32).astype(BF16)
    back_perm[...] = (time_of(rows) == cols).astype(F32).astype(BF16)
    x_copy.wait()
    project(wk, 0, their_rows)
    place_keys(their_rows, other)

    @pl.loop(n_chunks // 2, n_chunks)
    def _(c):
        forward(0, c, 0)

    project(wv, 1, their_rows)
    for c in range(n_chunks):
        lanes = slice(c * LANES, (c + 1) * LANES)
        vbuf[0, c] = jnp.dot(
            nat[1, :, lanes].T, fwd_perm[...], preferred_element_type=F32
        ).astype(BF16)

    @pl.loop(0, n_chunks)
    def _(c):
        forward(0, c, 1)

    def pass_keys(slot, first, last_):
        @pl.when(me >= slot)
        def _():
            @pl.loop(first, last_)
            def _(c):
                arrive(slot, c, 0)
                forward(slot, c, 0)

    pass_keys(2, 0, n_chunks // 2)

    local[3].wait()
    project(wq, 2, my_rows)
    project(wq, 2, their_rows)
    pass_keys(2, n_chunks // 2, n_chunks - 1)
    heads_per = LANES // HEAD_DIM
    for c in range(n_chunks):
        lanes = slice(c * LANES, (c + 1) * LANES)
        turned = jnp.dot(nat[2, :, lanes].T, fwd_perm[...], preferred_element_type=F32)
        turned = (turned * HEAD_DIM**-0.5).astype(BF16)
        for j in range(heads_per):
            for k in range(heads_per):
                piece = turned[k * HEAD_DIM : (k + 1) * HEAD_DIM]
                qz[c * heads_per + j, k * HEAD_DIM : (k + 1) * HEAD_DIM, :] = (
                    piece if j == k else jnp.zeros_like(piece)
                )

    pass_keys(2, n_chunks - 1, n_chunks)

    gap = time_of(cols) - time_of(rows)
    for slot in range(2):
        near_d[slot] = (gap + slot * length).astype(F32)
        near_c[slot] = log_multiplicity(gap + slot * length)
    key_step = lax.broadcasted_iota(jnp.int32, (per, per), 0)
    query_step = lax.broadcasted_iota(jnp.int32, (per, per), 1)
    for slot in range(2, n_slots):
        far_gap = classes * (query_step - key_step) + slot * length
        far_d[slot - 2] = far_gap.astype(F32)
        far_c[slot - 2] = log_multiplicity(far_gap)

    def slope_of(head, width):
        number = core * (n_chunks * heads_per) + head + 1
        exponent = jnp.full((1, width), number, jnp.int32).astype(F32)
        return jnp.exp2(exponent * (-ALIBI_EXP / HEADS))

    def attend(first, slot, c, j, key_rows, keys, queries, distance, logc):
        head = c * heads_per + j
        width = queries.stop - queries.start
        slope = slope_of(head, width)
        scores = jnp.dot(key_rows, qz[head, :, queries], preferred_element_type=F32)
        scores = scores + (logc - slope * distance)
        top = jnp.max(scores, axis=0, keepdims=True)
        if not first:
            before = m_ref[head, :, queries]
            top = jnp.maximum(top, before)
        weights = jnp.exp(scores - top)
        total = jnp.sum(weights, axis=0, keepdims=True)
        values = vbuf[slot, c, j * HEAD_DIM : (j + 1) * HEAD_DIM, keys]
        summed = jnp.dot(values, weights.astype(BF16), preferred_element_type=F32)
        if not first:
            fade = jnp.exp(before - top)
            total = total + fade * l_ref[head, :, queries]
            summed = summed + fade * acc[head, :, queries]
        m_ref[head, :, queries] = top
        l_ref[head, :, queries] = total
        acc[head, :, queries] = summed

    def dense(slot, c):
        tile = min(256, length)
        for j in range(heads_per):
            for q in range(length // tile):
                queries = slice(q * tile, (q + 1) * tile)
                attend(
                    slot == 0,
                    slot,
                    c,
                    j,
                    kbuf[slot, c].reshape(length, LANES),
                    slice(0, length),
                    queries,
                    near_d[slot, :, queries],
                    near_c[slot, :, queries],
                )

    def sparse(slot, c):
        for j in range(heads_per):
            for r in range(classes):
                span = slice(r * per, (r + 1) * per)
                key_rows = kbuf[slot, c, r].reshape(per, LANES)
                attend(False, slot, c, j, key_rows, span, span, far_d[slot - 2], far_c[slot - 2])

    @pl.loop(0, n_chunks)
    def _(c):
        dense(0, c)

        @pl.when(me >= 2)
        def _():
            arrive(2, c, 1)
            forward(2, c, 1)
            sparse(2, c)

    def relay(slot, close):
        @pl.when(me >= close)
        def _():
            arrive_keys(close)

        @pl.loop(0, n_chunks)
        def _(c):
            @pl.when(me >= slot)
            def _():
                arrive(slot, c, 0)
                forward(slot, c, 0)

            @pl.when(me >= close)
            def _():
                arrive(close, c, 1)
                dense(close, c) if close < 2 else sparse(close, c)

        @pl.when(me >= slot)
        def _():
            @pl.loop(0, n_chunks)
            def _(c):
                arrive(slot, c, 1)
                forward(slot, c, 1)
                sparse(slot, c)

    for slot in range(4, n_slots, 2):
        relay(slot, slot - 3)

    def finish(c):
        for j in range(heads_per):
            head = c * heads_per + j
            total = l_ref[head]
            hid[c, j * HEAD_DIM : (j + 1) * HEAD_DIM, :] = (acc[head] / total).astype(BF16)
            logs[head] = m_ref[head] + jnp.log(total)
        hid_nat[c] = (
            jnp.dot(hid[c], back_perm[...], preferred_element_type=F32).astype(BF16).T
        )

    def last(c):
        @pl.when(me >= hops - 1)
        def _():
            arrive(hops - 1, c, 1)
            sparse(hops - 1, c)

        finish(c)

    early = n_chunks - 1

    @pl.when(me >= hops - 1)
    def _():
        arrive_keys(hops - 1)

    @pl.loop(0, early)
    def _(c):
        last(c)

    local[4].wait()
    out_width = wo.shape[1]
    n_parts = p_send.shape[0]
    part_width = out_width // n_parts

    def all_parts():
        return [slice(p * part_width, (p + 1) * part_width) for p in range(n_parts)]

    sofar = jnp.concatenate([hid_nat[c] for c in range(early)], axis=1)
    for lanes in all_parts():
        part_sum[:, lanes] = jnp.dot(
            sofar, wo[: early * LANES, lanes], preferred_element_type=F32
        )
    last(early)

    part_copies = [
        pltpu.make_async_remote_copy(
            src_ref=part_send.at[:, lanes],
            dst_ref=part_recv.at[:, lanes],
            send_sem=p_send.at[p],
            recv_sem=p_recv.at[p],
            device_id={"tp": other},
        )
        for p, lanes in enumerate(all_parts())
    ]

    def partial(rows_, lanes):
        rest = jnp.dot(
            hid_nat[early, rows_, :], wo[early * LANES :, lanes], preferred_element_type=F32
        )
        return (part_sum[rows_, lanes] + rest).astype(BF16)

    for p, lanes in enumerate(all_parts()):
        part_send[:, lanes] = partial(their_rows, lanes)
        part_copies[p].start()
    log_sums[...] = jnp.dot(
        jnp.concatenate([logs[h] for h in range(logs.shape[0])], axis=0),
        back_perm[...].astype(F32),
        preferred_element_type=F32,
        precision=lax.Precision.HIGHEST,
    )
    for p, lanes in enumerate(all_parts()):
        own = partial(my_rows, lanes)
        part_copies[p].wait_recv()
        mixed[:, lanes] = (own.astype(F32) + part_recv[:, lanes].astype(F32)).astype(BF16)

    for copy in part_copies:
        copy.wait_send()
    for slot in range(1, n_slots):

        @pl.when(sends(slot))
        def _():
            @pl.loop(0, n_chunks)
            def _(c):
                for kind in range(2):
                    hop(slot, c, kind).wait_send()


def body(n_sp, tokens, w_query, w_key, w_value, w_out):
    half, depth = tokens.shape
    length = 2 * half
    width = w_query.shape[1]
    out_width = w_out.shape[1]
    heads = width // HEAD_DIM
    chunks = width // LANES
    slots = -(-REACH // length) + 1
    per = length // MIDDLE_DILATION
    parts = max(1, out_width // 512)
    hbm = pl.BlockSpec(memory_space=pl.ANY)
    vmem = pl.BlockSpec(memory_space=pltpu.VMEM)
    dma = pltpu.SemaphoreType.DMA
    return pl.pallas_call(
        functools.partial(kernel, n_sp),
        out_shape=(
            jax.ShapeDtypeStruct((half, out_width), BF16),
            jax.ShapeDtypeStruct((heads, length), F32),
        ),
        in_specs=[hbm] * 5,
        out_specs=(vmem, vmem),
        scratch_shapes=[
            pltpu.VMEM((length, depth), BF16),
            pltpu.VMEM((depth, width), BF16),
            pltpu.VMEM((depth, width), BF16),
            pltpu.VMEM((depth, width), BF16),
            pltpu.VMEM((width, out_width), BF16),
            pltpu.VMEM((3, length, width), BF16),
            pltpu.VMEM((slots, chunks, MIDDLE_DILATION, 2, per // 2, LANES), BF16),
            pltpu.VMEM((slots, chunks, LANES, length), BF16),
            pltpu.VMEM((heads, LANES, length), BF16),
            pltpu.VMEM((half, half), BF16),
            pltpu.VMEM((length, length), BF16),
            pltpu.VMEM((length, length), BF16),
            pltpu.VMEM((2, length, length), F32),
            pltpu.VMEM((2, length, length), F32),
            pltpu.VMEM((slots - 2, per, per), F32),
            pltpu.VMEM((slots - 2, per, per), F32),
            pltpu.VMEM((heads, 1, length), F32),
            pltpu.VMEM((heads, 1, length), F32),
            pltpu.VMEM((heads, HEAD_DIM, length), F32),
            pltpu.VMEM((chunks, LANES, length), BF16),
            pltpu.VMEM((chunks, length, LANES), BF16),
            pltpu.VMEM((heads, 1, length), F32),
            pltpu.VMEM((length, out_width), F32),
            pltpu.VMEM((half, out_width), BF16),
            pltpu.VMEM((half, out_width), BF16),
            dma((5,)),
            dma,
            dma,
            dma((slots - 1, chunks, 2)),
            dma((slots - 1, chunks, 2)),
            dma((parts,)),
            dma((parts,)),
        ],
        compiler_params=pltpu.CompilerParams(
            collective_id=0, has_side_effects=True, vmem_limit_bytes=60 * 1024 * 1024
        ),
        name="dilated_layer",
    )(tokens, w_query, w_key, w_value, w_out)


def solution(mesh):
    in_specs = (
        P(("grp", "sp", "tp"), None),
        P(None, "tp"),
        P(None, "tp"),
        P(None, "tp"),
        P("tp", None),
    )
    out_specs = (P(("grp", "sp", "tp"), None), P("tp", ("grp", "sp")))
    return jax.shard_map(
        functools.partial(body, mesh.shape["sp"]),
        mesh=mesh,
        in_specs=in_specs,
        out_specs=out_specs,
        check_vma=False,
    )
```

profile of v0, /device:TPU:17, one launch (start us, length us, event | category | flops | bytes accessed | tf_op | source)
XLA Modules:
  0.0 65.1 jit_solution(12488691763846092578)
XLA Ops:
  0.6 61.5 %dilated_layer.1 = (bf16[256,2048]{1,0:T(8,128)(2,1)}, f32[8,512]{1,0:T(8,128)}) custom-call(bf16[256,2048]{1,0:T(8,128)(2,1)} %tokens.1, bf16[2048,512]{1,0:T(8,128)(2,1)} %w_query.1, bf16[2048,512]{1,0:T(8,128)(2,1)} %w_key.1, bf16[2048,512]{1,0:T(8,128)(2,1)} %w_value.1, bf16[512,2048]{1,0:T(8,128)(2,1)} %w_out.1), custom_call_target="tpu_custom_call" | custom-call | tf_op jit(solution)/shard_map/dilated_layer/pallas_call | solution.py:465
  62.1 0.0 copy-start
  62.1 2.3 %copy.9 = bf16[256,2048]{1,0:T(8,128)(2,1)} copy(bf16[256,2048]{1,0:T(8,128)(2,1)} %get-tuple-element.4) | data formatting | bytes 2097152
  64.5 0.0 copy-done
  64.5 0.6 copy.10
Async XLA Ops:
  62.1 2.3 %copy-start = (f32[8,512]{1,0:T(8,128)S(1)}, f32[8,512]{1,0:T(8,128)}, u32[]{:S(2)}) copy-start(f32[8,512]{1,0:T(8,128)} %get-tuple-element.5) | copy-start | bytes 49156
where the time goes:
time: 65.2 us; the launch traced here: 65.1 us
  Pallas kernels  61.5 us (94%)
  local copies, waits for them, and re-layouts  2.92 us (4%)
    pallas_call x1, Pallas kernels, body(): pl.pallas_call(functools.partial(kernel, n_sp), out_shape=(jax.ShapeDtype...  61.5 us
    unnamed x4, local copies, waits for them, and re-layouts  2.92 us

commit v1 on v0

v1 whole, which is shorter than its diff:
```python
import functools
import math

import jax
import jax.numpy as jnp
from jax import lax
from jax.experimental import pallas as pl
from jax.experimental.pallas import tpu as pltpu
from jax.sharding import PartitionSpec as P

HEADS = 16
HEAD_DIM = 64
WINDOW_KEY_STEPS = 128
MIDDLE_DILATION = 4
FAR_DILATION = 16
REACH = 2048
ALIBI_EXP = 16.0
LANES = 128
ONES = 16
F32 = jnp.float32
BF16 = jnp.bfloat16
FAR, UP, OWN = 0, 1, 2


def log_multiplicity(distance):
    def window(stride):
        inside = (distance >= 0) & (distance <= WINDOW_KEY_STEPS * stride)
        if stride > 1:
            inside = inside & ((distance & (stride - 1)) == 0)
        return inside.astype(jnp.int32)

    count = window(1) + window(MIDDLE_DILATION) + window(FAR_DILATION)
    return jnp.where(
        count == 3,
        math.log(3.0),
        jnp.where(count == 2, math.log(2.0), jnp.where(count == 1, 0.0, -jnp.inf)),
    ).astype(F32)


def kernel(
    n_sp,
    tokens,
    w_query,
    w_key,
    w_value,
    w_out,
    mixed,
    log_sums,
    xin,
    x,
    wq,
    wk,
    wv,
    wo,
    nat,
    kbuf,
    vbuf,
    vtail,
    qbuf,
    half_perm,
    back_perm,
    tail_pick,
    tab,
    m_ref,
    l_ref,
    acc,
    o_out,
    s_out,
    o_in,
    s_in,
    hid,
    hid_nat,
    logs,
    part_sum,
    part_send,
    part_recv,
    local_sem,
    x_send,
    x_recv,
    kv_send,
    kv_recv,
    q_send,
    q_recv,
    o_send,
    o_recv,
    p_send,
    p_recv,
):
    half, depth = tokens.shape
    length = 2 * half
    n_chunks = kbuf.shape[1]
    classes = MIDDLE_DILATION
    per = length // classes
    per_half = per // 2
    me = lax.axis_index("sp")
    core = lax.axis_index("tp")
    other = 1 - core
    odd = lax.rem(me, 2)
    mate = me + 1 - 2 * odd
    is_even = odd == 0
    is_odd = odd == 1
    has_up = me + 2 < n_sp
    has_far = me + 4 < n_sp
    has_down = me >= 2
    up = jnp.where(has_up, me + 2, me - 2)
    down = jnp.where(has_down, me - 2, me + 2)

    local = [
        pltpu.make_async_copy(tokens, xin, local_sem.at[0]),
        pltpu.make_async_copy(w_key, wk, local_sem.at[1]),
        pltpu.make_async_copy(w_query, wq, local_sem.at[2]),
        pltpu.make_async_copy(w_value, wv, local_sem.at[3]),
        pltpu.make_async_copy(w_out, wo, local_sem.at[4]),
    ]
    for copy in local[:4]:
        copy.start()

    barrier = pltpu.get_barrier_semaphore()
    pl.semaphore_signal(barrier, inc=1, device_id={"tp": other})
    pl.semaphore_signal(barrier, inc=1, device_id={"sp": mate})

    @pl.when(has_up)
    def _():
        pl.semaphore_signal(barrier, inc=1, device_id={"sp": me + 2})

    @pl.when(has_down)
    def _():
        pl.semaphore_signal(barrier, inc=1, device_id={"sp": me - 2})

    half_rows = lax.broadcasted_iota(jnp.int32, (half, half), 0)
    half_cols = lax.broadcasted_iota(jnp.int32, (half, half), 1)
    half_bits = per_half.bit_length() - 1
    half_time = classes * (half_rows & (per_half - 1)) + (half_rows >> half_bits)
    half_perm[...] = (half_time == half_cols).astype(F32).astype(BF16)

    peers = 2 + jnp.where(has_up, 1, 0) + jnp.where(has_down, 1, 0)
    pl.semaphore_wait(barrier, peers)

    local[0].wait()
    x[:, core] = (
        jnp.dot(half_perm[...], xin[...], preferred_element_type=F32)
        .astype(BF16)
        .reshape(classes, per_half, depth)
    )
    x_copy = pltpu.make_async_remote_copy(
        src_ref=x.at[:, core],
        dst_ref=x.at[:, core],
        send_sem=x_send,
        recv_sem=x_recv,
        device_id={"tp": other},
    )
    x_copy.start()

    def project(weights, side):
        rows = x[:, side].reshape(half, depth)
        return jnp.dot(rows, weights[...], preferred_element_type=F32)

    def place_keys(side):
        keys = project(wk, side).astype(BF16)
        for c in range(n_chunks):
            piece = keys[:, c * LANES : (c + 1) * LANES]
            kbuf[0, c, :, side] = piece.reshape(classes, per_half, LANES)

    def place_queries(side):
        queries = (project(wq, side) * HEAD_DIM**-0.5).astype(BF16)
        nat[0, :, side] = queries.reshape(classes, per_half, queries.shape[1])

    def place_values(side):
        values = project(wv, side).astype(BF16)
        nat[1, :, side] = values.reshape(classes, per_half, values.shape[1])

    def key_copy(c, late):
        side = core + late * (1 - 2 * core)
        return pltpu.make_async_remote_copy(
            src_ref=kbuf.at[0, c, :, side],
            dst_ref=kbuf.at[1, c, :, side],
            send_sem=kv_send.at[c, late],
            recv_sem=kv_recv.at[c, late],
            device_id={"sp": mate},
        )

    def value_copy(c):
        return pltpu.make_async_remote_copy(
            src_ref=vbuf.at[0, c],
            dst_ref=vbuf.at[1, c],
            send_sem=kv_send.at[c, 2],
            recv_sem=kv_recv.at[c, 2],
            device_id={"sp": mate},
        )

    def query_copy(c, relay):
        return pltpu.make_async_remote_copy(
            src_ref=qbuf.at[relay, c],
            dst_ref=qbuf.at[relay + 1, c],
            send_sem=q_send.at[relay, c],
            recv_sem=q_recv.at[relay, c],
            device_id={"sp": down},
        )

    def out_copies(kind, c):
        return [
            pltpu.make_async_remote_copy(
                src_ref=src.at[kind, c],
                dst_ref=dst.at[kind, c],
                send_sem=o_send.at[kind, c, i],
                recv_sem=o_recv.at[kind, c, i],
                device_id={"sp": up},
            )
            for i, (src, dst) in enumerate(((o_out, o_in), (s_out, s_in)))
        ]

    def turned(which, c):
        lanes = slice(c * LANES, (c + 1) * LANES)
        return nat[which].reshape(length, n_chunks * LANES)[:, lanes].T

    local[1].wait()
    place_keys(core)
    early = n_chunks // 2
    for c in range(early):
        key_copy(c, 0).start()
    local[2].wait()
    place_queries(core)
    local[3].wait()
    local[4].start()
    place_values(core)

    x_copy.wait()
    place_queries(other)
    for c in range(n_chunks):
        qbuf[0, c] = turned(0, c)
        if c < early:

            @pl.when(has_down)
            def _():
                query_copy(c, 0).start()

    place_keys(other)
    for c in range(early):
        key_copy(c, 1).start()
    place_values(other)
    for c in range(n_chunks):
        if c >= early:
            key_copy(c, 0).start()
            key_copy(c, 1).start()
        vbuf[0, c] = turned(1, c)
        value_copy(c).start()

    key_step = lax.broadcasted_iota(jnp.int32, (per, per), 0)
    query_step = lax.broadcasted_iota(jnp.int32, (per, per), 1)
    tail = per // classes
    tail_bits = tail.bit_length() - 1
    heads_per = LANES // HEAD_DIM

    def slope_of(head):
        number = core * (n_chunks * heads_per) + head + 1
        exponent = jnp.full((1, per), number, jnp.int32).astype(F32)
        return jnp.exp2(exponent * (-ALIBI_EXP / HEADS))

    slopes = [slope_of(h) for h in range(n_chunks * heads_per)]

    def fill(first_row, distance, logc):
        gap = distance.astype(F32)
        rows = pl.ds(pl.multiple_of(first_row, per), per)
        for h in range(n_chunks * heads_per):
            c, j = divmod(h, heads_per)
            tab[c, rows, j * per : (j + 1) * per] = logc - slopes[h] * gap

    steps = classes * (query_step - key_step)
    T0 = 0
    T_CLASS = (2 * classes - 1) * per
    T_TAIL = T_CLASS + classes * per

    @pl.loop(0, 2 * classes - 1)
    def _(e):
        distance = steps + (classes - 1 - e)
        fill(T0 + e * per, distance, log_multiplicity(distance))

    @pl.loop(0, classes)
    def _(e):
        distance = steps + (e + 1) * length
        fill(T_CLASS + e * per, distance, log_multiplicity(distance))

    tail_class = key_step >> tail_bits
    tail_step = (key_step & (tail - 1)) + (per - tail)

    @pl.loop(0, classes)
    def _(r):
        distance = length + classes * (query_step - tail_step) + (r - tail_class)
        logc = jnp.where(tail_class == r, -jnp.inf, log_multiplicity(distance))
        fill(T_TAIL + r * per, distance, logc)

    rows = lax.broadcasted_iota(jnp.int32, (length, length), 0)
    cols = lax.broadcasted_iota(jnp.int32, (length, length), 1)
    per_bits = per.bit_length() - 1
    time_of_row = classes * (rows & (per - 1)) + (rows >> per_bits)
    back_perm[...] = (time_of_row == cols).astype(F32).astype(BF16)
    pick_rows = lax.broadcasted_iota(jnp.int32, (length, per), 0)
    pick_cols = lax.broadcasted_iota(jnp.int32, (length, per), 1)
    pick = (pick_cols >> tail_bits) * per + (per - tail) + (pick_cols & (tail - 1))
    tail_pick[...] = (pick_rows == pick).astype(F32).astype(BF16)

    ones_of = functools.partial(jnp.ones, dtype=BF16)

    def class_part(slot, c, r, table):
        keys = kbuf[slot, c, r].reshape(per, LANES)
        bias = tab[c, table : table + per, :]
        return keys, bias, vbuf[slot, c, :, r * per : (r + 1) * per]

    def gap_table(blocks):
        return T_CLASS + (blocks - 1) * per

    def tail_part(c, r):
        last = tail + per_half - per
        keys = jnp.concatenate(
            [kbuf[1, c, k, 1, per_half - tail :, :] for k in range(classes)], axis=0
        )
        table = T_TAIL + r * per
        return keys, tab[c, table : table + per, :], vtail[c]

    def own_part(c, r):
        first = T0 + (classes - 1 - r) * per
        return (
            kbuf[0, c].reshape(length, LANES),
            tab[c, first : first + length, :],
            vbuf[0, c],
        )

    def attend(item, c, q_slot, parts_of):
        for r in range(classes):
            lanes = slice(r * per, (r + 1) * per)
            parts = parts_of(r)
            first = qbuf[q_slot, c, :HEAD_DIM, lanes]
            second = qbuf[q_slot, c, HEAD_DIM:, lanes]
            blank = jnp.zeros_like(first)
            queries = jnp.concatenate(
                [
                    jnp.concatenate([first, blank], axis=0),
                    jnp.concatenate([blank, second], axis=0),
                ],
                axis=1,
            )
            scores = [
                jnp.dot(keys, queries, preferred_element_type=F32) + bias
                for keys, bias, _ in parts
            ]
            tops = [jnp.max(s, axis=0, keepdims=True) for s in scores]
            top = functools.reduce(jnp.maximum, tops)
            weights = jnp.concatenate(
                [jnp.exp(s - top).astype(BF16) for s in scores], axis=0
            )
            values = jnp.concatenate([v for _, _, v in parts], axis=1)
            count = values.shape[1]
            for j in range(heads_per):
                mine = values[j * HEAD_DIM : (j + 1) * HEAD_DIM]
                summed = jnp.dot(
                    jnp.concatenate([mine, ones_of((ONES, count))], axis=0),
                    weights[:, j * per : (j + 1) * per],
                    preferred_element_type=F32,
                )
                row = slice(r * heads_per + j, r * heads_per + j + 1)
                acc[item, c, j * HEAD_DIM : (j + 1) * HEAD_DIM, lanes] = summed[:HEAD_DIM]
                l_ref[item, c, row, :] = summed[HEAD_DIM : HEAD_DIM + 1]
                m_ref[item, c, row, :] = top[:, j * per : (j + 1) * per]

    def pieces():
        for r in range(classes):
            for j in range(heads_per):
                row = slice(r * heads_per + j, r * heads_per + j + 1)
                dims = slice(j * HEAD_DIM, (j + 1) * HEAD_DIM)
                yield row, dims, slice(r * per, (r + 1) * per)

    def take_in(item, c, kind):
        for copy in out_copies(kind, c):
            copy.wait_recv()
        here, there = m_ref[item, c], s_in[kind, c]
        top = jnp.maximum(here, there)
        keep, gain = jnp.exp(here - top), jnp.exp(there - top)
        m_ref[item, c] = top
        l_ref[item, c] = keep * l_ref[item, c] + gain
        for row, dims, lanes in pieces():
            acc[item, c, dims, lanes] = (
                keep[row] * acc[item, c, dims, lanes]
                + gain[row] * o_in[kind, c, dims, lanes].astype(F32)
            )

    def level(item, c, out):
        total = l_ref[item, c]
        scale = 1.0 / total
        for row, dims, lanes in pieces():
            out[dims, lanes] = (acc[item, c, dims, lanes] * scale[row]).astype(BF16)
        return m_ref[item, c] + jnp.log(total)

    def emit(item, c):
        s_out[item, c] = level(item, c, o_out.at[item, c])
        for copy in out_copies(item, c):
            copy.start()

    def finish(c):
        @pl.when(has_down)
        def _():
            take_in(OWN, c, UP)

        logs[c] = level(OWN, c, hid.at[c])
        hid_nat[c] = (
            jnp.dot(hid[c], back_perm[...], preferred_element_type=F32).astype(BF16).T
        )

    def merge_up(c):
        @pl.when(has_up)
        def _():
            @pl.when(has_down)
            def _():
                take_in(UP, c, FAR)

            emit(UP, c)

    def step(c):
        @pl.when(has_up)
        def _():
            query_copy(c, 0).wait_recv()

            @pl.when(has_down)
            def _():
                query_copy(c, 1).start()

        @pl.when(has_down & (c + early < n_chunks))
        def _():
            query_copy(c + early, 0).start()

        key_copy(c, 0).wait_recv()
        key_copy(c, 1).wait_recv()
        value_copy(c).wait_recv()
        vtail[c] = jnp.dot(
            vbuf[1, c], tail_pick[...], preferred_element_type=F32
        ).astype(BF16)

        @pl.when(has_up & is_even)
        def _():
            attend(
                UP,
                c,
                1,
                lambda r: [
                    class_part(0, c, r, gap_table(2)),
                    class_part(1, c, r, gap_table(1)),
                    tail_part(c, r),
                ],
            )

        @pl.when(has_up & is_odd)
        def _():
            attend(
                UP,
                c,
                1,
                lambda r: [
                    class_part(0, c, r, gap_table(2)),
                    class_part(1, c, r, gap_table(3)),
                ],
            )

        @pl.when(is_even)
        def _():
            attend(OWN, c, 0, lambda r: [own_part(c, r)])

        @pl.when(is_odd)
        def _():
            attend(
                OWN,
                c,
                0,
                lambda r: [
                    own_part(c, r),
                    class_part(1, c, r, gap_table(1)),
                    tail_part(c, r),
                ],
            )

        @pl.when(c >= 1)
        def _():
            merge_up(c - 1)

        @pl.when(has_far)
        def _():
            query_copy(c, 1).wait_recv()

            @pl.when(is_even)
            def _():
                attend(
                    FAR,
                    c,
                    2,
                    lambda r: [
                        class_part(0, c, r, gap_table(4)),
                        class_part(1, c, r, gap_table(3)),
                    ],
                )

            @pl.when(is_odd)
            def _():
                attend(FAR, c, 2, lambda r: [class_part(0, c, r, gap_table(4))])

            emit(FAR, c)

        @pl.when(c >= 2)
        def _():
            finish(c - 2)

    @pl.loop(0, n_chunks)
    def _(c):
        step(c)

    local[4].wait()
    out_width = wo.shape[1]
    n_parts = p_send.shape[0]
    part_width = out_width // n_parts
    done = n_chunks - 2

    def all_parts():
        return [slice(p * part_width, (p + 1) * part_width) for p in range(n_parts)]

    sofar = jnp.concatenate([hid_nat[c] for c in range(done)], axis=1)
    for lanes in all_parts():
        part_sum[:, lanes] = jnp.dot(
            sofar, wo[: done * LANES, lanes], preferred_element_type=F32
        )
    merge_up(n_chunks - 1)
    for c in range(done, n_chunks):
        finish(c)

    part_copies = [
        pltpu.make_async_remote_copy(
            src_ref=part_send.at[:, lanes],
            dst_ref=part_recv.at[:, lanes],
            send_sem=p_send.at[p],
            recv_sem=p_recv.at[p],
            device_id={"tp": other},
        )
        for p, lanes in enumerate(all_parts())
    ]
    my_rows = pl.ds(pl.multiple_of(core * half, half), half)
    their_rows = pl.ds(pl.multiple_of(other * half, half), half)

    def partial(rows_, lanes):
        late = jnp.concatenate([hid_nat[c, rows_, :] for c in range(done, n_chunks)], axis=1)
        rest = jnp.dot(late, wo[done * LANES :, lanes], preferred_element_type=F32)
        return (part_sum[rows_, lanes] + rest).astype(BF16)

    for p, lanes in enumerate(all_parts()):
        part_send[:, lanes] = partial(their_rows, lanes)
        part_copies[p].start()

    ordered = jnp.concatenate(
        [
            jnp.concatenate(
                [logs[c, r * heads_per + j : r * heads_per + j + 1, :] for r in range(classes)],
                axis=1,
            )
            for c in range(n_chunks)
            for j in range(heads_per)
        ],
        axis=0,
    )
    high = ordered.astype(BF16)
    left = ordered - high.astype(F32)
    middle = left.astype(BF16)
    low = (left - middle.astype(F32)).astype(BF16)
    log_sums[...] = functools.reduce(
        jnp.add,
        [
            jnp.dot(piece, back_perm[...], preferred_element_type=F32)
            for piece in (low, middle, high)
        ],
    )
    for p, lanes in enumerate(all_parts()):
        own = partial(my_rows, lanes)
        part_copies[p].wait_recv()
        mixed[:, lanes] = (own.astype(F32) + part_recv[:, lanes].astype(F32)).astype(BF16)

    for copy in part_copies:
        copy.wait_send()

    @pl.loop(0, n_chunks)
    def _(c):
        key_copy(c, 0).wait_send()
        key_copy(c, 1).wait_send()
        value_copy(c).wait_send()

        @pl.when(has_down)
        def _():
            query_copy(c, 0).wait_send()

        @pl.when(has_down & has_up)
        def _():
            query_copy(c, 1).wait_send()

        @pl.when(has_far)
        def _():
            for copy in out_copies(FAR, c):
                copy.wait_send()

        @pl.when(has_up)
        def _():
            for copy in out_copies(UP, c):
                copy.wait_send()


def body(n_sp, tokens, w_query, w_key, w_value, w_out):
    half, depth = tokens.shape
    length = 2 * half
    width = w_query.shape[1]
    out_width = w_out.shape[1]
    heads = width // HEAD_DIM
    chunks = width // LANES
    assert REACH == MIDDLE_DILATION * length and n_sp % 2 == 0
    per = length // MIDDLE_DILATION
    stats = MIDDLE_DILATION * (LANES // HEAD_DIM)
    parts = max(1, out_width // 512)
    tables = (4 * MIDDLE_DILATION - 1) * per
    hbm = pl.BlockSpec(memory_space=pl.ANY)
    vmem = pl.BlockSpec(memory_space=pltpu.VMEM)
    dma = pltpu.SemaphoreType.DMA
    return pl.pallas_call(
        functools.partial(kernel, n_sp),
        out_shape=(
            jax.ShapeDtypeStruct((half, out_width), BF16),
            jax.ShapeDtypeStruct((heads, length), F32),
        ),
        in_specs=[hbm] * 5,
        out_specs=(vmem, vmem),
        scratch_shapes=[
            pltpu.VMEM((half, depth), BF16),
            pltpu.VMEM((MIDDLE_DILATION, 2, per // 2, depth), BF16),
            pltpu.VMEM((depth, width), BF16),
            pltpu.VMEM((depth, width), BF16),
            pltpu.VMEM((depth, width), BF16),
            pltpu.VMEM((width, out_width), BF16),
            pltpu.VMEM((2, MIDDLE_DILATION, 2, per // 2, width), BF16),
            pltpu.VMEM((2, chunks, MIDDLE_DILATION, 2, per // 2, LANES), BF16),
            pltpu.VMEM((2, chunks, LANES, length), BF16),
            pltpu.VMEM((chunks, LANES, per), BF16),
            pltpu.VMEM((3, chunks, LANES, length), BF16),
            pltpu.VMEM((half, half), BF16),
            pltpu.VMEM((length, length), BF16),
            pltpu.VMEM((length, per), BF16),
            pltpu.VMEM((chunks, tables, 2 * per), F32),
            pltpu.VMEM((3, chunks, stats, per), F32),
            pltpu.VMEM((3, chunks, stats, per), F32),
            pltpu.VMEM((3, chunks, LANES, length), F32),
            pltpu.VMEM((2, chunks, LANES, length), BF16),
            pltpu.VMEM((2, chunks, stats, per), F32),
            pltpu.VMEM((2, chunks, LANES, length), BF16),
            pltpu.VMEM((2, chunks, stats, per), F32),
            pltpu.VMEM((chunks, LANES, length), BF16),
            pltpu.VMEM((chunks, length, LANES), BF16),
            pltpu.VMEM((chunks, stats, per), F32),
            pltpu.VMEM((length, out_width), F32),
            pltpu.VMEM((half, out_width), BF16),
            pltpu.VMEM((half, out_width), BF16),
            dma((5,)),
            dma,
            dma,
            dma((chunks, 3)),
            dma((chunks, 3)),
            dma((2, chunks)),
            dma((2, chunks)),
            dma((2, chunks, 2)),
            dma((2, chunks, 2)),
            dma((parts,)),
            dma((parts,)),
        ],
        compiler_params=pltpu.CompilerParams(
            collective_id=0, has_side_effects=True, vmem_limit_bytes=60 * 1024 * 1024
        ),
        name="dilated_layer",
    )(tokens, w_query, w_key, w_value, w_out)


def solution(mesh):
    in_specs = (
        P(("grp", "sp", "tp"), None),
        P(None, "tp"),
        P(None, "tp"),
        P(None, "tp"),
        P("tp", None),
    )
    out_specs = (P(("grp", "sp", "tp"), None), P("tp", ("grp", "sp")))
    return jax.shard_map(
        functools.partial(body, mesh.shape["sp"]),
        mesh=mesh,
        in_specs=in_specs,
        out_specs=out_specs,
        check_vma=False,
    )
```

time: 65.2 us -> 55 us (0.84)
  Pallas kernels: 61.5 us -> 51.3 us
    pallas_call x1, Pallas kernels: 61.5 us -> 51.3 us  [body(): pl.pallas_call(functools.partial(kernel, n_sp), out_shape=(jax.ShapeDtype...]
where the time goes in v1:
time: 55 us; the launch traced here: 54.8 us
  Pallas kernels  51.3 us (93%)
  local copies, waits for them, and re-layouts  2.92 us (5%)
  between operations  0.65 us (1%)
    pallas_call x1, Pallas kernels, body(): pl.pallas_call(functools.partial(kernel, n_sp), out_shape=(jax.ShapeDtype...  51.3 us
    unnamed x4, local copies, waits for them, and re-layouts  2.92 us

profile of v1, /device:TPU:17, one launch (start us, length us, event | category | flops | bytes accessed | tf_op | source)
XLA Modules:
  0.0 54.8 jit_solution(17447537327346918820)
XLA Ops:
  0.6 51.3 %dilated_layer.1 = (bf16[256,2048]{1,0:T(8,128)(2,1)}, f32[8,512]{1,0:T(8,128)}) custom-call(bf16[256,2048]{1,0:T(8,128)(2,1)} %tokens.1, bf16[2048,512]{1,0:T(8,128)(2,1)} %w_query.1, bf16[2048,512]{1,0:T(8,128)(2,1)} %w_key.1, bf16[2048,512]{1,0:T(8,128)(2,1)} %w_value.1, bf16[512,2048]{1,0:T(8,128)(2,1)} %w_out.1), custom_call_target="tpu_custom_call" | custom-call | tf_op jit(solution)/shard_map/dilated_layer/pallas_call | solution.py:623
  51.9 0.0 copy-start
  51.9 2.3 %copy.9 = bf16[256,2048]{1,0:T(8,128)(2,1)} copy(bf16[256,2048]{1,0:T(8,128)(2,1)} %get-tuple-element.4) | data formatting | bytes 2097152
  54.2 0.0 copy-done
  54.2 0.6 %copy.10 = f32[8,512]{1,0:T(8,128)} copy(f32[8,512]{1,0:T(8,128)S(1)} %copy-done) | data formatting | bytes 32768
Async XLA Ops:
  51.9 2.3 %copy-start = (f32[8,512]{1,0:T(8,128)S(1)}, f32[8,512]{1,0:T(8,128)}, u32[]{:S(2)}) copy-start(f32[8,512]{1,0:T(8,128)} %get-tuple-element.5) | copy-start | bytes 49156

commit v2 on v1

--- a/solution.py
+++ b/solution.py
@@ -71,9 +71,8 @@
     hid,
     hid_nat,
     logs,
+    hid_in,
     part_sum,
-    part_send,
-    part_recv,
     local_sem,
     x_send,
     x_recv,
@@ -83,8 +82,10 @@
     q_recv,
     o_send,
     o_recv,
-    p_send,
-    p_recv,
+    h_send,
+    h_recv,
+    w_send,
+    w_recv,
 ):
     half, depth = tokens.shape
     length = 2 * half
@@ -110,7 +111,7 @@
         pltpu.make_async_copy(w_key, wk, local_sem.at[1]),
         pltpu.make_async_copy(w_query, wq, local_sem.at[2]),
         pltpu.make_async_copy(w_value, wv, local_sem.at[3]),
-        pltpu.make_async_copy(w_out, wo, local_sem.at[4]),
+        pltpu.make_async_copy(w_out, wo.at[0], local_sem.at[4]),
     ]
     for copy in local[:4]:
         copy.start()
@@ -132,9 +133,6 @@
     half_bits = per_half.bit_length() - 1
     half_time = classes * (half_rows & (per_half - 1)) + (half_rows >> half_bits)
     half_perm[...] = (half_time == half_cols).astype(F32).astype(BF16)
-
-    peers = 2 + jnp.where(has_up, 1, 0) + jnp.where(has_down, 1, 0)
-    pl.semaphore_wait(barrier, peers)
 
     local[0].wait()
     x[:, core] = (
@@ -142,6 +140,8 @@
         .astype(BF16)
         .reshape(classes, per_half, depth)
     )
+    peers = 2 + jnp.where(has_up, 1, 0) + jnp.where(has_down, 1, 0)
+    pl.semaphore_wait(barrier, peers)
     x_copy = pltpu.make_async_remote_copy(
         src_ref=x.at[:, core],
         dst_ref=x.at[:, core],
@@ -150,6 +150,8 @@
         device_id={"tp": other},
     )
     x_copy.start()
+    my_rows = pl.ds(pl.multiple_of(core * half, half), half)
+    their_rows = pl.ds(pl.multiple_of(other * half, half), half)
 
     def project(weights, side):
         rows = x[:, side].reshape(half, depth)
@@ -188,26 +190,43 @@
             device_id={"sp": mate},
         )
 
-    def query_copy(c, relay):
+    def query_copy(s, relay):
         return pltpu.make_async_remote_copy(
-            src_ref=qbuf.at[relay, c],
-            dst_ref=qbuf.at[relay + 1, c],
-            send_sem=q_send.at[relay, c],
-            recv_sem=q_recv.at[relay, c],
+            src_ref=qbuf.at[relay, s],
+            dst_ref=qbuf.at[relay + 1, s],
+            send_sem=q_send.at[relay, s],
+            recv_sem=q_recv.at[relay, s],
             device_id={"sp": down},
         )
 
-    def out_copies(kind, c):
+    def out_copies(kind, s):
         return [
             pltpu.make_async_remote_copy(
-                src_ref=src.at[kind, c],
-                dst_ref=dst.at[kind, c],
-                send_sem=o_send.at[kind, c, i],
-                recv_sem=o_recv.at[kind, c, i],
+                src_ref=src.at[kind, s],
+                dst_ref=dst.at[kind, s],
+                send_sem=o_send.at[kind, s, i],
+                recv_sem=o_recv.at[kind, s, i],
                 device_id={"sp": up},
             )
             for i, (src, dst) in enumerate(((o_out, o_in), (s_out, s_in)))
         ]
+
+    def hidden_copy(c):
+        return pltpu.make_async_remote_copy(
+            src_ref=hid_nat.at[c, their_rows],
+            dst_ref=hid_in.at[c],
+            send_sem=h_send.at[c],
+            recv_sem=h_recv.at[c],
+            device_id={"tp": other},
+        )
+
+    w_copy = pltpu.make_async_remote_copy(
+        src_ref=w_out,
+        dst_ref=wo.at[1],
+        send_sem=w_send,
+        recv_sem=w_recv,
+        device_id={"tp": other},
+    )
 
     def turned(which, c):
         lanes = slice(c * LANES, (c + 1) * LANES)
@@ -226,13 +245,17 @@
 
     x_copy.wait()
     place_queries(other)
+    groups = 2
+    wide = length // groups
     for c in range(n_chunks):
-        qbuf[0, c] = turned(0, c)
-        if c < early:
-
-            @pl.when(has_down)
-            def _():
-                query_copy(c, 0).start()
+        queries = turned(0, c)
+        for g in range(groups):
+            qbuf[0, c * groups + g] = queries[:, g * wide : (g + 1) * wide]
+            if c == 0:
+
+                @pl.when(has_down)
+                def _():
+                    query_copy(g, 0).start()
 
     place_keys(other)
     for c in range(early):
@@ -244,6 +267,7 @@
             key_copy(c, 1).start()
         vbuf[0, c] = turned(1, c)
         value_copy(c).start()
+    w_copy.start()
 
     key_step = lax.broadcasted_iota(jnp.int32, (per, per), 0)
     query_step = lax.broadcasted_iota(jnp.int32, (per, per), 1)
@@ -310,7 +334,6 @@
         return T_CLASS + (blocks - 1) * per
 
     def tail_part(c, r):
-        last = tail + per_half - per
         keys = jnp.concatenate(
             [kbuf[1, c, k, 1, per_half - tail :, :] for k in range(classes)], axis=0
         )
@@ -325,12 +348,16 @@
             vbuf[0, c],
         )
 
-    def attend(item, c, q_slot, parts_of):
-        for r in range(classes):
-            lanes = slice(r * per, (r + 1) * per)
+    per_group = classes // groups
+
+    def attend(item, c, g, q_slot, parts_of):
+        piece = c * groups + g
+        for i in range(per_group):
+            r = g * per_group + i
+            lanes = slice(i * per, (i + 1) * per)
             parts = parts_of(r)
-            first = qbuf[q_slot, c, :HEAD_DIM, lanes]
-            second = qbuf[q_slot, c, HEAD_DIM:, lanes]
+            first = qbuf[q_slot, piece, :HEAD_DIM, lanes]
+            second = qbuf[q_slot, piece, HEAD_DIM:, lanes]
             blank = jnp.zeros_like(first)
             queries = jnp.concatenate(
                 [
@@ -357,88 +384,97 @@
                     weights[:, j * per : (j + 1) * per],
                     preferred_element_type=F32,
                 )
-                row = slice(r * heads_per + j, r * heads_per + j + 1)
-                acc[item, c, j * HEAD_DIM : (j + 1) * HEAD_DIM, lanes] = summed[:HEAD_DIM]
-                l_ref[item, c, row, :] = summed[HEAD_DIM : HEAD_DIM + 1]
-                m_ref[item, c, row, :] = top[:, j * per : (j + 1) * per]
-
-    def pieces():
-        for r in range(classes):
+                row = slice(i * heads_per + j, i * heads_per + j + 1)
+                acc[item, piece, j * HEAD_DIM : (j + 1) * HEAD_DIM, lanes] = summed[:HEAD_DIM]
+                l_ref[item, piece, row, :] = summed[HEAD_DIM : HEAD_DIM + 1]
+                m_ref[item, piece, row, :] = top[:, j * per : (j + 1) * per]
+
+    def blocks():
+        for i in range(per_group):
             for j in range(heads_per):
-                row = slice(r * heads_per + j, r * heads_per + j + 1)
+                row = slice(i * heads_per + j, i * heads_per + j + 1)
                 dims = slice(j * HEAD_DIM, (j + 1) * HEAD_DIM)
-                yield row, dims, slice(r * per, (r + 1) * per)
-
-    def take_in(item, c, kind):
-        for copy in out_copies(kind, c):
+                yield row, dims, slice(i * per, (i + 1) * per)
+
+    def take_in(item, s, kind):
+        for copy in out_copies(kind, s):
             copy.wait_recv()
-        here, there = m_ref[item, c], s_in[kind, c]
+        here, there = m_ref[item, s], s_in[kind, s]
         top = jnp.maximum(here, there)
         keep, gain = jnp.exp(here - top), jnp.exp(there - top)
-        m_ref[item, c] = top
-        l_ref[item, c] = keep * l_ref[item, c] + gain
-        for row, dims, lanes in pieces():
-            acc[item, c, dims, lanes] = (
-                keep[row] * acc[item, c, dims, lanes]
-                + gain[row] * o_in[kind, c, dims, lanes].astype(F32)
-            )
-
-    def level(item, c, out):
-        total = l_ref[item, c]
+        m_ref[item, s] = top
+        l_ref[item, s] = keep * l_ref[item, s] + gain
+        for row, dims, lanes in blocks():
+            acc[item, s, dims, lanes] = (
+                keep[row] * acc[item, s, dims, lanes]
+                + gain[row] * o_in[kind, s, dims, lanes].astype(F32)
+            )
+
+    def level(item, s, out):
+        total = l_ref[item, s]
         scale = 1.0 / total
-        for row, dims, lanes in pieces():
-            out[dims, lanes] = (acc[item, c, dims, lanes] * scale[row]).astype(BF16)
-        return m_ref[item, c] + jnp.log(total)
-
-    def emit(item, c):
-        s_out[item, c] = level(item, c, o_out.at[item, c])
-        for copy in out_copies(item, c):
+        for row, dims, lanes in blocks():
+            out[dims, lanes] = (acc[item, s, dims, lanes] * scale[row]).astype(BF16)
+        return m_ref[item, s] + jnp.log(total)
+
+    def emit(item, s):
+        s_out[item, s] = level(item, s, o_out.at[item, s])
+        for copy in out_copies(item, s):
             copy.start()
 
-    def finish(c):
+    def finish(c, g):
+        piece = c * groups + g
+
         @pl.when(has_down)
         def _():
-            take_in(OWN, c, UP)
-
-        logs[c] = level(OWN, c, hid.at[c])
-        hid_nat[c] = (
-            jnp.dot(hid[c], back_perm[...], preferred_element_type=F32).astype(BF16).T
-        )
-
-    def merge_up(c):
-        @pl.when(has_up)
+            take_in(OWN, piece, UP)
+
+        logs[piece] = level(OWN, piece, hid.at[c, :, g * wide : (g + 1) * wide])
+        if g == groups - 1:
+            hid_nat[c] = (
+                jnp.dot(hid[c], back_perm[...], preferred_element_type=F32).astype(BF16).T
+            )
+            hidden_copy(c).start()
+
+    n_pieces = n_chunks * groups
+
+    def merge_up(s):
+        @pl.when(has_up & (s >= 0) & (s < n_pieces))
         def _():
             @pl.when(has_down)
             def _():
-                take_in(UP, c, FAR)
-
-            emit(UP, c)
-
-    def step(c):
-        @pl.when(has_up)
-        def _():
-            query_copy(c, 0).wait_recv()
+                take_in(UP, s, FAR)
+
+            emit(UP, s)
+
+    def pass_on(s):
+        @pl.when(has_up & (s < n_pieces))
+        def _():
+            query_copy(s, 0).wait_recv()
 
             @pl.when(has_down)
             def _():
-                query_copy(c, 1).start()
-
-        @pl.when(has_down & (c + early < n_chunks))
-        def _():
-            query_copy(c + early, 0).start()
-
-        key_copy(c, 0).wait_recv()
-        key_copy(c, 1).wait_recv()
-        value_copy(c).wait_recv()
-        vtail[c] = jnp.dot(
-            vbuf[1, c], tail_pick[...], preferred_element_type=F32
-        ).astype(BF16)
+                query_copy(s, 1).start()
+
+        @pl.when(has_down & (s + groups < n_pieces))
+        def _():
+            query_copy(s + groups, 0).start()
+
+    def attend_all(c, g):
+        if g == 0:
+            key_copy(c, 0).wait_recv()
+            key_copy(c, 1).wait_recv()
+            value_copy(c).wait_recv()
+            vtail[c] = jnp.dot(
+                vbuf[1, c], tail_pick[...], preferred_element_type=F32
+            ).astype(BF16)
 
         @pl.when(has_up & is_even)
         def _():
             attend(
                 UP,
                 c,
+                g,
                 1,
                 lambda r: [
                     class_part(0, c, r, gap_table(2)),
@@ -452,6 +488,7 @@
             attend(
                 UP,
                 c,
+                g,
                 1,
                 lambda r: [
                     class_part(0, c, r, gap_table(2)),
@@ -461,13 +498,14 @@
 
         @pl.when(is_even)
         def _():
-            attend(OWN, c, 0, lambda r: [own_part(c, r)])
+            attend(OWN, c, g, 0, lambda r: [own_part(c, r)])
 
         @pl.when(is_odd)
         def _():
             attend(
                 OWN,
                 c,
+                g,
                 0,
                 lambda r: [
                     own_part(c, r),
@@ -476,19 +514,17 @@
                 ],
             )
 
-        @pl.when(c >= 1)
-        def _():
-            merge_up(c - 1)
-
         @pl.when(has_far)
         def _():
-            query_copy(c, 1).wait_recv()
+            piece = c * groups + g
+            query_copy(piece, 1).wait_recv()
 
             @pl.when(is_even)
             def _():
                 attend(
                     FAR,
                     c,
+                    g,
                     2,
                     lambda r: [
                         class_part(0, c, r, gap_table(4)),
@@ -498,62 +534,72 @@
 
             @pl.when(is_odd)
             def _():
-                attend(FAR, c, 2, lambda r: [class_part(0, c, r, gap_table(4))])
-
-            emit(FAR, c)
-
-        @pl.when(c >= 2)
-        def _():
-            finish(c - 2)
-
-    @pl.loop(0, n_chunks)
+                attend(FAR, c, g, 2, lambda r: [class_part(0, c, r, gap_table(4))])
+
+            emit(FAR, piece)
+
+    @pl.loop(0, n_chunks + 1)
     def _(c):
-        step(c)
-
-    local[4].wait()
-    out_width = wo.shape[1]
-    n_parts = p_send.shape[0]
+        for g in range(groups):
+            beat = c * groups + g
+            pass_on(beat)
+            merge_up(beat - 3)
+            if g == 0:
+
+                @pl.when(c >= 1)
+                def _():
+                    attend_all(c - 1, groups - 1)
+
+            else:
+
+                @pl.when(c < n_chunks)
+                def _():
+                    attend_all(c, g - 1)
+
+            @pl.when(c >= 2)
+            def _():
+                finish(c - 2, g)
+
+    out_width = wo.shape[2]
+    n_parts = max(1, out_width // 512)
     part_width = out_width // n_parts
-    done = n_chunks - 2
+    done = n_chunks - 1
 
     def all_parts():
         return [slice(p * part_width, (p + 1) * part_width) for p in range(n_parts)]
 
-    sofar = jnp.concatenate([hid_nat[c] for c in range(done)], axis=1)
+    def spread(first, last_):
+        return jnp.concatenate(
+            [hid_nat[c, my_rows, :] for c in range(first, last_)]
+            + [hid_in[c] for c in range(first, last_)],
+            axis=1,
+        )
+
+    def weights_of(first, last_, lanes):
+        rows_ = slice(first * LANES, last_ * LANES)
+        return jnp.concatenate([wo[0, rows_, lanes], wo[1, rows_, lanes]], axis=0)
+
+    merge_up(n_pieces - 1)
+    local[4].wait()
+    w_copy.wait()
+    for c in range(done):
+        hidden_copy(c).wait_recv()
+    sofar = spread(0, done)
     for lanes in all_parts():
         part_sum[:, lanes] = jnp.dot(
-            sofar, wo[: done * LANES, lanes], preferred_element_type=F32
+            sofar, weights_of(0, done, lanes), preferred_element_type=F32
         )
-    merge_up(n_chunks - 1)
-    for c in range(done, n_chunks):
-        finish(c)
-
-    part_copies = [
-        pltpu.make_async_remote_copy(
-            src_ref=part_send.at[:, lanes],
-            dst_ref=part_recv.at[:, lanes],
-            send_sem=p_send.at[p],
-            recv_sem=p_recv.at[p],
-            device_id={"tp": other},
-        )
-        for p, lanes in enumerate(all_parts())
-    ]
-    my_rows = pl.ds(pl.multiple_of(core * half, half), half)
-    their_rows = pl.ds(pl.multiple_of(other * half, half), half)
-
-    def partial(rows_, lanes):
-        late = jnp.concatenate([hid_nat[c, rows_, :] for c in range(done, n_chunks)], axis=1)
-        rest = jnp.dot(late, wo[done * LANES :, lanes], preferred_element_type=F32)
-        return (part_sum[rows_, lanes] + rest).astype(BF16)
-
-    for p, lanes in enumerate(all_parts()):
-        part_send[:, lanes] = partial(their_rows, lanes)
-        part_copies[p].start()
+    for g in range(groups):
+        finish(done, g)
 
     ordered = jnp.concatenate(
         [
             jnp.concatenate(
-                [logs[c, r * heads_per + j : r * heads_per + j + 1, :] for r in range(classes)],
+                [
+                    logs[c * groups + g, i * heads_per + j : i * heads_per + j + 1, :]
+                    for g in range(groups)
+                    for i in range(per_group)
+                ],
                 axis=1,
             )
             for c in range(n_chunks)
@@ -572,36 +618,38 @@
             for piece in (low, middle, high)
         ],
     )
-    for p, lanes in enumerate(all_parts()):
-        own = partial(my_rows, lanes)
-        part_copies[p].wait_recv()
-        mixed[:, lanes] = (own.astype(F32) + part_recv[:, lanes].astype(F32)).astype(BF16)
-
-    for copy in part_copies:
-        copy.wait_send()
+    for c in range(done, n_chunks):
+        hidden_copy(c).wait_recv()
+    late = spread(done, n_chunks)
+    for lanes in all_parts():
+        rest = jnp.dot(late, weights_of(done, n_chunks, lanes), preferred_element_type=F32)
+        mixed[:, lanes] = (part_sum[:, lanes] + rest).astype(BF16)
 
     @pl.loop(0, n_chunks)
     def _(c):
         key_copy(c, 0).wait_send()
         key_copy(c, 1).wait_send()
         value_copy(c).wait_send()
-
+        hidden_copy(c).wait_send()
+
+    @pl.loop(0, n_pieces)
+    def _(s):
         @pl.when(has_down)
         def _():
-            query_copy(c, 0).wait_send()
+            query_copy(s, 0).wait_send()
 
         @pl.when(has_down & has_up)
         def _():
-            query_copy(c, 1).wait_send()
+            query_copy(s, 1).wait_send()
 
         @pl.when(has_far)
         def _():
-            for copy in out_copies(FAR, c):
+            for copy in out_copies(FAR, s):
                 copy.wait_send()
 
         @pl.when(has_up)
         def _():
-            for copy in out_copies(UP, c):
+            for copy in out_copies(UP, s):
                 copy.wait_send()
 
 
@@ -614,8 +662,9 @@
     chunks = width // LANES
     assert REACH == MIDDLE_DILATION * length and n_sp % 2 == 0
     per = length // MIDDLE_DILATION
-    stats = MIDDLE_DILATION * (LANES // HEAD_DIM)
-    parts = max(1, out_width // 512)
+    groups = 2
+    pieces, wide = chunks * groups, length // groups
+    stats = MIDDLE_DILATION // groups * (LANES // HEAD_DIM)
     tables = (4 * MIDDLE_DILATION - 1) * per
     hbm = pl.BlockSpec(memory_space=pl.ANY)
     vmem = pl.BlockSpec(memory_space=pltpu.VMEM)
@@ -634,43 +683,44 @@
             pltpu.VMEM((depth, width), BF16),
             pltpu.VMEM((depth, width), BF16),
             pltpu.VMEM((depth, width), BF16),
-            pltpu.VMEM((width, out_width), BF16),
+            pltpu.VMEM((2, width, out_width), BF16),
             pltpu.VMEM((2, MIDDLE_DILATION, 2, per // 2, width), BF16),
             pltpu.VMEM((2, chunks, MIDDLE_DILATION, 2, per // 2, LANES), BF16),
             pltpu.VMEM((2, chunks, LANES, length), BF16),
             pltpu.VMEM((chunks, LANES, per), BF16),
-            pltpu.VMEM((3, chunks, LANES, length), BF16),
+            pltpu.VMEM((3, pieces, LANES, wide), BF16),
             pltpu.VMEM((half, half), BF16),
             pltpu.VMEM((length, length), BF16),
             pltpu.VMEM((length, per), BF16),
             pltpu.VMEM((chunks, tables, 2 * per), F32),
-            pltpu.VMEM((3, chunks, stats, per), F32),
-            pltpu.VMEM((3, chunks, stats, per), F32),
-            pltpu.VMEM((3, chunks, LANES, length), F32),
-            pltpu.VMEM((2, chunks, LANES, length), BF16),
-            pltpu.VMEM((2, chunks, stats, per), F32),
-            pltpu.VMEM((2, chunks, LANES, length), BF16),
-            pltpu.VMEM((2, chunks, stats, per), F32),
+            pltpu.VMEM((3, pieces, stats, per), F32),
+            pltpu.VMEM((3, pieces, stats, per), F32),
+            pltpu.VMEM((3, pieces, LANES, wide), F32),
+            pltpu.VMEM((2, pieces, LANES, wide), BF16),
+            pltpu.VMEM((2, pieces, stats, per), F32),
+            pltpu.VMEM((2, pieces, LANES, wide), BF16),
+            pltpu.VMEM((2, pieces, stats, per), F32),
             pltpu.VMEM((chunks, LANES, length), BF16),
             pltpu.VMEM((chunks, length, LANES), BF16),
-            pltpu.VMEM((chunks, stats, per), F32),
-            pltpu.VMEM((length, out_width), F32),
-            pltpu.VMEM((half, out_width), BF16),
-            pltpu.VMEM((half, out_width), BF16),
+            pltpu.VMEM((pieces, stats, per), F32),
+            pltpu.VMEM((chunks, half, LANES), BF16),
+            pltpu.VMEM((half, out_width), F32),
             dma((5,)),
             dma,
             dma,
             dma((chunks, 3)),
             dma((chunks, 3)),
-            dma((2, chunks)),
-            dma((2, chunks)),
-            dma((2, chunks, 2)),
-            dma((2, chunks, 2)),
-            dma((parts,)),
-            dma((parts,)),
+            dma((2, pieces)),
+            dma((2, pieces)),
+            dma((2, pieces, 2)),
+            dma((2, pieces, 2)),
+            dma((chunks,)),
+            dma((chunks,)),
+            dma,
+            dma,
         ],
         compiler_params=pltpu.CompilerParams(
-            collective_id=0, has_side_effects=True, vmem_limit_bytes=60 * 1024 * 1024
+            collective_id=0, has_side_effects=True, vmem_limit_bytes=52 * 1024 * 1024
         ),
         name="dilated_layer",
     )(tokens, w_query, w_key, w_value, w_out)

time: 55 us -> 48.1 us (0.87)
  Pallas kernels: 51.3 us -> 45.8 us
  local copies, waits for them, and re-layouts: 2.92 us -> 1.58 us
    pallas_call x1, Pallas kernels: 51.3 us -> 45.8 us  [body(): pl.pallas_call(functools.partial(kernel, n_sp), out_shape=(jax.ShapeDtype...]
    unnamed x4 -> x2, local copies, waits for them, and re-layouts: 2.92 us -> 1.58 us
where the time goes in v2:
time: 48.1 us; the launch traced here: 48 us
  Pallas kernels  45.8 us (95%)
  local copies, waits for them, and re-layouts  1.58 us (3%)
  between operations  0.64 us (1%)
    pallas_call x1, Pallas kernels, body(): pl.pallas_call(functools.partial(kernel, n_sp), out_shape=(jax.ShapeDtype...  45.8 us
    unnamed x2, local copies, waits for them, and re-layouts  1.58 us

profile of v2, /device:TPU:17, one launch (start us, length us, event | category | flops | bytes accessed | tf_op | source)
XLA Modules:
  0.0 48.0 jit_solution(6376309558645091822)
XLA Ops:
  0.6 45.8 %dilated_layer.1 = (bf16[256,2048]{1,0:T(8,128)(2,1)S(1)}, f32[8,512]{1,0:T(8,128)S(1)}) custom-call(bf16[256,2048]{1,0:T(8,128)(2,1)} %tokens.1, bf16[2048,512]{1,0:T(8,128)(2,1)} %w_query.1, bf16[2048,512]{1,0:T(8,128)(2,1)} %w_key.1, bf16[2048,512]{1,0:T(8,128)(2,1)} %w_value.1, bf16[512,2048]{1,0:T(8,128)(2,1)} %w_out.1), custom_call_target="tpu_custom_call" | custom-call | tf_op jit(solution)/shard_map/dilated_layer/pallas_call | solution.py:672
  46.4 1.0 %copy.9 = bf16[256,2048]{1,0:T(8,128)(2,1)} copy(bf16[256,2048]{1,0:T(8,128)(2,1)S(1)} %get-tuple-element.4) | data formatting | bytes 2097152
  47.4 0.6 %copy.10 = f32[8,512]{1,0:T(8,128)} copy(f32[8,512]{1,0:T(8,128)S(1)} %get-tuple-element.5) | data formatting | bytes 32768

commit v3 on v2

--- a/solution.py
+++ b/solution.py
@@ -258,12 +258,12 @@
                     query_copy(g, 0).start()
 
     place_keys(other)
-    for c in range(early):
-        key_copy(c, 1).start()
+    key_copy(0, 1).start()
     place_values(other)
     for c in range(n_chunks):
         if c >= early:
             key_copy(c, 0).start()
+        if c >= 1:
             key_copy(c, 1).start()
         vbuf[0, c] = turned(1, c)
         value_copy(c).start()
@@ -350,44 +350,56 @@
 
     per_group = classes // groups
 
-    def attend(item, c, g, q_slot, parts_of):
+    def score(c, g, i, q_slot, parts_of):
         piece = c * groups + g
+        lanes = slice(i * per, (i + 1) * per)
+        parts = parts_of(g * per_group + i)
+        first = qbuf[q_slot, piece, :HEAD_DIM, lanes]
+        second = qbuf[q_slot, piece, HEAD_DIM:, lanes]
+        blank = jnp.zeros_like(first)
+        queries = jnp.concatenate(
+            [
+                jnp.concatenate([first, blank], axis=0),
+                jnp.concatenate([blank, second], axis=0),
+            ],
+            axis=1,
+        )
+        scores = [
+            jnp.dot(keys, queries, preferred_element_type=F32) + bias
+            for keys, bias, _ in parts
+        ]
+        tops = [jnp.max(s, axis=0, keepdims=True) for s in scores]
+        values = jnp.concatenate([v for _, _, v in parts], axis=1)
+        return scores, functools.reduce(jnp.maximum, tops), values
+
+    def weigh(item, c, g, i, scores, top, values):
+        piece = c * groups + g
+        lanes = slice(i * per, (i + 1) * per)
+        weights = jnp.concatenate(
+            [jnp.exp(s - top).astype(BF16) for s in scores], axis=0
+        )
+        count = values.shape[1]
+        for j in range(heads_per):
+            mine = values[j * HEAD_DIM : (j + 1) * HEAD_DIM]
+            summed = jnp.dot(
+                jnp.concatenate([mine, ones_of((ONES, count))], axis=0),
+                weights[:, j * per : (j + 1) * per],
+                preferred_element_type=F32,
+            )
+            row = slice(i * heads_per + j, i * heads_per + j + 1)
+            acc[item, piece, j * HEAD_DIM : (j + 1) * HEAD_DIM, lanes] = summed[:HEAD_DIM]
+            l_ref[item, piece, row, :] = summed[HEAD_DIM : HEAD_DIM + 1]
+            m_ref[item, piece, row, :] = top[:, j * per : (j + 1) * per]
+
+    def attend(c, g, items):
+        held = None
         for i in range(per_group):
-            r = g * per_group + i
-            lanes = slice(i * per, (i + 1) * per)
-            parts = parts_of(r)
-            first = qbuf[q_slot, piece, :HEAD_DIM, lanes]
-            second = qbuf[q_slot, piece, HEAD_DIM:, lanes]
-            blank = jnp.zeros_like(first)
-            queries = jnp.concatenate(
-                [
-                    jnp.concatenate([first, blank], axis=0),
-                    jnp.concatenate([blank, second], axis=0),
-                ],
-                axis=1,
-            )
-            scores = [
-                jnp.dot(keys, queries, preferred_element_type=F32) + bias
-                for keys, bias, _ in parts
-            ]
-            tops = [jnp.max(s, axis=0, keepdims=True) for s in scores]
-            top = functools.reduce(jnp.maximum, tops)
-            weights = jnp.concatenate(
-                [jnp.exp(s - top).astype(BF16) for s in scores], axis=0
-            )
-            values = jnp.concatenate([v for _, _, v in parts], axis=1)
-            count = values.shape[1]
-            for j in range(heads_per):
-                mine = values[j * HEAD_DIM : (j + 1) * HEAD_DIM]
-                summed = jnp.dot(
-                    jnp.concatenate([mine, ones_of((ONES, count))], axis=0),
-                    weights[:, j * per : (j + 1) * per],
-                    preferred_element_type=F32,
-                )
-                row = slice(i * heads_per + j, i * heads_per + j + 1)
-                acc[item, piece, j * HEAD_DIM : (j + 1) * HEAD_DIM, lanes] = summed[:HEAD_DIM]
-                l_ref[item, piece, row, :] = summed[HEAD_DIM : HEAD_DIM + 1]
-                m_ref[item, piece, row, :] = top[:, j * per : (j + 1) * per]
+            for item, q_slot, parts_of in items:
+                scored = (item, c, g, i, *score(c, g, i, q_slot, parts_of))
+                if held is not None:
+                    weigh(*held)
+                held = scored
+        weigh(*held)
 
     def blocks():
         for i in range(per_group):
@@ -469,74 +481,79 @@
                 vbuf[1, c], tail_pick[...], preferred_element_type=F32
             ).astype(BF16)
 
-        @pl.when(has_up & is_even)
-        def _():
-            attend(
-                UP,
-                c,
-                g,
-                1,
-                lambda r: [
-                    class_part(0, c, r, gap_table(2)),
-                    class_part(1, c, r, gap_table(1)),
-                    tail_part(c, r),
-                ],
-            )
-
-        @pl.when(has_up & is_odd)
-        def _():
-            attend(
-                UP,
-                c,
-                g,
-                1,
-                lambda r: [
-                    class_part(0, c, r, gap_table(2)),
-                    class_part(1, c, r, gap_table(3)),
-                ],
-            )
-
-        @pl.when(is_even)
-        def _():
-            attend(OWN, c, g, 0, lambda r: [own_part(c, r)])
-
-        @pl.when(is_odd)
-        def _():
-            attend(
-                OWN,
-                c,
-                g,
-                0,
-                lambda r: [
-                    own_part(c, r),
-                    class_part(1, c, r, gap_table(1)),
-                    tail_part(c, r),
-                ],
-            )
+        piece = c * groups + g
 
         @pl.when(has_far)
         def _():
-            piece = c * groups + g
             query_copy(piece, 1).wait_recv()
 
             @pl.when(is_even)
             def _():
                 attend(
-                    FAR,
                     c,
                     g,
-                    2,
-                    lambda r: [
-                        class_part(0, c, r, gap_table(4)),
-                        class_part(1, c, r, gap_table(3)),
+                    [
+                        (
+                            FAR,
+                            2,
+                            lambda r: [
+                                class_part(0, c, r, gap_table(4)),
+                                class_part(1, c, r, gap_table(3)),
+                            ],
+                        ),
                     ],
                 )
 
             @pl.when(is_odd)
             def _():
-                attend(FAR, c, g, 2, lambda r: [class_part(0, c, r, gap_table(4))])
+                attend(c, g, [(FAR, 2, lambda r: [class_part(0, c, r, gap_table(4))])])
 
             emit(FAR, piece)
+
+        @pl.when(is_even)
+        def _():
+            attend(
+                c,
+                g,
+                [
+                    (
+                        UP,
+                        1,
+                        lambda r: [
+                            class_part(0, c, r, gap_table(2)),
+                            class_part(1, c, r, gap_table(1)),
+                            tail_part(c, r),
+                        ],
+                    ),
+                    (OWN, 0, lambda r: [own_part(c, r)]),
+                ],
+            )
+
+        @pl.when(is_odd)
+        def _():
+            attend(
+                c,
+                g,
+                [
+                    (
+                        UP,
+                        1,
+                        lambda r: [
+                            class_part(0, c, r, gap_table(2)),
+                            class_part(1, c, r, gap_table(3)),
+                        ],
+                    ),
+                    (
+                        OWN,
+                        0,
+                        lambda r: [
+                            own_part(c, r),
+                            class_part(1, c, r, gap_table(1)),
+                            tail_part(c, r),
+                        ],
+                    ),
+                ],
+            )
 
     @pl.loop(0, n_chunks + 1)
     def _(c):

time: 48.1 us -> 46.3 us (0.963)
  Pallas kernels: 45.8 us -> 43.8 us
    pallas_call x1, Pallas kernels: 45.8 us -> 43.8 us  [body(): pl.pallas_call(functools.partial(kernel, n_sp), out_shape=(jax.ShapeDtype...]
where the time goes in v3:
time: 46.3 us; the launch traced here: 46 us
  Pallas kernels  43.8 us (95%)
  local copies, waits for them, and re-layouts  1.58 us (3%)
  between operations  0.64 us (1%)
    pallas_call x1, Pallas kernels, body(): pl.pallas_call(functools.partial(kernel, n_sp), out_shape=(jax.ShapeDtype...  43.8 us
    unnamed x2, local copies, waits for them, and re-layouts  1.58 us

profile of v3, /device:TPU:17, one launch (start us, length us, event | category | flops | bytes accessed | tf_op | source)
XLA Modules:
  0.0 46.0 jit_solution(18358075804961979203)
XLA Ops:
  0.6 43.8 %dilated_layer.1 = (bf16[256,2048]{1,0:T(8,128)(2,1)S(1)}, f32[8,512]{1,0:T(8,128)S(1)}) custom-call(bf16[256,2048]{1,0:T(8,128)(2,1)} %tokens.1, bf16[2048,512]{1,0:T(8,128)(2,1)} %w_query.1, bf16[2048,512]{1,0:T(8,128)(2,1)} %w_key.1, bf16[2048,512]{1,0:T(8,128)(2,1)} %w_value.1, bf16[512,2048]{1,0:T(8,128)(2,1)} %w_out.1), custom_call_target="tpu_custom_call" | custom-call | tf_op jit(solution)/shard_map/dilated_layer/pallas_call | solution.py:689
  44.4 1.0 %copy.9 = bf16[256,2048]{1,0:T(8,128)(2,1)} copy(bf16[256,2048]{1,0:T(8,128)(2,1)S(1)} %get-tuple-element.4) | data formatting | bytes 2097152
  45.4 0.6 %copy.10 = f32[8,512]{1,0:T(8,128)} copy(f32[8,512]{1,0:T(8,128)S(1)} %get-tuple-element.5) | data formatting | bytes 32768

commit v4 on v3

--- a/solution.py
+++ b/solution.py
@@ -267,7 +267,6 @@
             key_copy(c, 1).start()
         vbuf[0, c] = turned(1, c)
         value_copy(c).start()
-    w_copy.start()
 
     key_step = lax.broadcasted_iota(jnp.int32, (per, per), 0)
     query_step = lax.broadcasted_iota(jnp.int32, (per, per), 1)
@@ -560,6 +559,12 @@
         for g in range(groups):
             beat = c * groups + g
             pass_on(beat)
+            if g == 0:
+
+                @pl.when(c == 2)
+                def _():
+                    w_copy.start()
+
             merge_up(beat - 3)
             if g == 0:
 
@@ -670,6 +675,17 @@
                 copy.wait_send()
 
 
+def deliver(mixed, log_sums, mixed_out, log_sums_out, sems):
+    copies = [
+        pltpu.make_async_copy(mixed, mixed_out, sems.at[0]),
+        pltpu.make_async_copy(log_sums, log_sums_out, sems.at[1]),
+    ]
+    for copy in copies:
+        copy.start()
+    for copy in copies:
+        copy.wait()
+
+
 def body(n_sp, tokens, w_query, w_key, w_value, w_out):
     half, depth = tokens.shape
     length = 2 * half
@@ -686,7 +702,7 @@
     hbm = pl.BlockSpec(memory_space=pl.ANY)
     vmem = pl.BlockSpec(memory_space=pltpu.VMEM)
     dma = pltpu.SemaphoreType.DMA
-    return pl.pallas_call(
+    results = pl.pallas_call(
         functools.partial(kernel, n_sp),
         out_shape=(
             jax.ShapeDtypeStruct((half, out_width), BF16),
@@ -741,6 +757,15 @@
         ),
         name="dilated_layer",
     )(tokens, w_query, w_key, w_value, w_out)
+    return pl.pallas_call(
+        deliver,
+        out_shape=tuple(jax.ShapeDtypeStruct(r.shape, r.dtype) for r in results),
+        in_specs=[vmem, vmem],
+        out_specs=(hbm, hbm),
+        scratch_shapes=[dma((2,))],
+        compiler_params=pltpu.CompilerParams(vmem_limit_bytes=8 * 1024 * 1024),
+        name="deliver",
+    )(*results)
 
 
 def solution(mesh):

time: 46.3 us -> 45.7 us (0.987)
  local copies, waits for them, and re-layouts: 1.58 us -> 0 us
  Pallas kernels: 43.8 us -> 44.8 us
    unnamed x2 -> x0, local copies, waits for them, and re-layouts: 1.58 us -> none
    pallas_call x0 -> x1, Pallas kernels: none -> 0.99 us  [body(): pl.pallas_call(deliver, out_shape=tuple((jax.ShapeDtypeStruct(r.shape, r....]
where the time goes in v4:
time: 45.7 us; the launch traced here: 45.4 us
  Pallas kernels  44.8 us (98%)
  between operations  0.64 us (1%)
    pallas_call x1, Pallas kernels, body(): pl.pallas_call(functools.partial(kernel, n_sp), out_shape=(jax.ShapeDtype...  43.8 us
    pallas_call x1, Pallas kernels, body(): pl.pallas_call(deliver, out_shape=tuple((jax.ShapeDtypeStruct(r.shape, r....  0.99 us

profile of v4, /device:TPU:17, one launch (start us, length us, event | category | flops | bytes accessed | tf_op | source)
XLA Modules:
  0.0 45.4 jit_solution(13208282042435788595)
XLA Ops:
  0.6 43.8 %dilated_layer.1 = (bf16[256,2048]{1,0:T(8,128)(2,1)S(1)}, f32[8,512]{1,0:T(8,128)S(1)}) custom-call(bf16[256,2048]{1,0:T(8,128)(2,1)} %tokens.1, bf16[2048,512]{1,0:T(8,128)(2,1)} %w_query.1, bf16[2048,512]{1,0:T(8,128)(2,1)} %w_key.1, bf16[2048,512]{1,0:T(8,128)(2,1)} %w_value.1, bf16[512,2048]{1,0:T(8,128)(2,1)} %w_out.1), custom_call_target="tpu_custom_call" | custom-call | tf_op jit(solution)/shard_map/dilated_layer/pallas_call | solution.py:705
  44.4 1.0 %deliver.1 = (bf16[256,2048]{1,0:T(8,128)(2,1)}, f32[8,512]{1,0:T(8,128)}) custom-call(bf16[256,2048]{1,0:T(8,128)(2,1)S(1)} %get-tuple-element.4.mixed, f32[8,512]{1,0:T(8,128)S(1)} %get-tuple-element.5.log_sums), custom_call_target="tpu_custom_call" | custom-call | tf_op jit(solution)/shard_map/deliver/pallas_call | solution.py:760

commit v5 on v4

--- a/solution.py
+++ b/solution.py
@@ -142,14 +142,18 @@
     )
     peers = 2 + jnp.where(has_up, 1, 0) + jnp.where(has_down, 1, 0)
     pl.semaphore_wait(barrier, peers)
-    x_copy = pltpu.make_async_remote_copy(
-        src_ref=x.at[:, core],
-        dst_ref=x.at[:, core],
-        send_sem=x_send,
-        recv_sem=x_recv,
-        device_id={"tp": other},
-    )
-    x_copy.start()
+    x_copies = [
+        pltpu.make_async_remote_copy(
+            src_ref=x.at[pl.ds(first, classes // 2), core],
+            dst_ref=x.at[pl.ds(first, classes // 2), core],
+            send_sem=x_send.at[i],
+            recv_sem=x_recv.at[i],
+            device_id={"tp": other},
+        )
+        for i, first in enumerate((0, classes // 2))
+    ]
+    for copy in x_copies:
+        copy.start()
     my_rows = pl.ds(pl.multiple_of(core * half, half), half)
     their_rows = pl.ds(pl.multiple_of(other * half, half), half)
 
@@ -163,9 +167,13 @@
             piece = keys[:, c * LANES : (c + 1) * LANES]
             kbuf[0, c, :, side] = piece.reshape(classes, per_half, LANES)
 
-    def place_queries(side):
-        queries = (project(wq, side) * HEAD_DIM**-0.5).astype(BF16)
-        nat[0, :, side] = queries.reshape(classes, per_half, queries.shape[1])
+    def place_queries(side, first=0, count=classes):
+        rows = x[first : first + count, side].reshape(count * per_half, depth)
+        queries = jnp.dot(rows, wq[...], preferred_element_type=F32)
+        queries = (queries * HEAD_DIM**-0.5).astype(BF16)
+        nat[0, first : first + count, side] = queries.reshape(
+            count, per_half, queries.shape[1]
+        )
 
     def place_values(side):
         values = project(wv, side).astype(BF16)
@@ -243,14 +251,16 @@
     local[4].start()
     place_values(core)
 
-    x_copy.wait()
-    place_queries(other)
     groups = 2
     wide = length // groups
-    for c in range(n_chunks):
-        queries = turned(0, c)
-        for g in range(groups):
-            qbuf[0, c * groups + g] = queries[:, g * wide : (g + 1) * wide]
+    per_group = classes // groups
+    for g in range(groups):
+        x_copies[g].wait()
+        place_queries(other, g * per_group, per_group)
+        for c in range(n_chunks):
+            lanes = slice(c * LANES, (c + 1) * LANES)
+            rows = nat[0, g * per_group : (g + 1) * per_group, :, :, lanes]
+            qbuf[0, c * groups + g] = rows.reshape(wide, LANES).T
             if c == 0:
 
                 @pl.when(has_down)
@@ -346,8 +356,6 @@
             tab[c, first : first + length, :],
             vbuf[0, c],
         )
-
-    per_group = classes // groups
 
     def score(c, g, i, q_slot, parts_of):
         piece = c * groups + g
@@ -739,8 +747,8 @@
             pltpu.VMEM((chunks, half, LANES), BF16),
             pltpu.VMEM((half, out_width), F32),
             dma((5,)),
-            dma,
-            dma,
+            dma((2,)),
+            dma((2,)),
             dma((chunks, 3)),
             dma((chunks, 3)),
             dma((2, pieces)),

time: 45.7 us -> 45.6 us (level)
  no operation moved by 1% of the time
where the time goes in v5:
time: 45.6 us; the launch traced here: 45.4 us
  Pallas kernels  44.7 us (98%)
  between operations  0.64 us (1%)
    pallas_call x1, Pallas kernels, body(): pl.pallas_call(functools.partial(kernel, n_sp), out_shape=(jax.ShapeDtype...  43.7 us
    pallas_call x1, Pallas kernels, body(): pl.pallas_call(deliver, out_shape=tuple((jax.ShapeDtypeStruct(r.shape, r....  0.99 us

profile of v5, /device:TPU:17, one launch (start us, length us, event | category | flops | bytes accessed | tf_op | source)
XLA Modules:
  0.0 45.4 jit_solution(5541890396491310426)
XLA Ops:
  0.6 43.7 %dilated_layer.1 = (bf16[256,2048]{1,0:T(8,128)(2,1)S(1)}, f32[8,512]{1,0:T(8,128)S(1)}) custom-call(bf16[256,2048]{1,0:T(8,128)(2,1)} %tokens.1, bf16[2048,512]{1,0:T(8,128)(2,1)} %w_query.1, bf16[2048,512]{1,0:T(8,128)(2,1)} %w_key.1, bf16[2048,512]{1,0:T(8,128)(2,1)} %w_value.1, bf16[512,2048]{1,0:T(8,128)(2,1)} %w_out.1), custom_call_target="tpu_custom_call" | custom-call | tf_op jit(solution)/shard_map/dilated_layer/pallas_call | solution.py:713
  44.4 1.0 %deliver.1 = (bf16[256,2048]{1,0:T(8,128)(2,1)}, f32[8,512]{1,0:T(8,128)}) custom-call(bf16[256,2048]{1,0:T(8,128)(2,1)S(1)} %get-tuple-element.4.mixed, f32[8,512]{1,0:T(8,128)S(1)} %get-tuple-element.5.log_sums), custom_call_target="tpu_custom_call" | custom-call | tf_op jit(solution)/shard_map/deliver/pallas_call | solution.py:768
